TPU v7x, 32 devices: a whole 2x2x4 slice. The times are simulated.
32 devices in a mesh: sp: 16 (over z, y, x), tp: 2 (over core).
Axes of the slice: x: 2, y: 2, z: 4, core: 2. Of those that a mesh axis runs over, the one named last changes fastest.
Arguments:
- resid: bfloat16 [3072, 2048], P('sp'), may hold values from -6 to 6
- query: bfloat16 [3072, 2048], P('sp', 'tp'), may hold values from -6 to 6
- key: bfloat16 [3072, 1024], P('sp', 'tp'), may hold values from -6 to 6
- value: bfloat16 [3072, 1024], P('sp', 'tp'), may hold values from -6 to 6
- q_gain: float32 [128], replicated, may hold values from 0.3 to 5, as said below
- k_gain: float32 [128], replicated, may hold values from 0.3 to 5, as said below
- out_weight: bfloat16 [2048, 2048], P('tp'), may hold values from -0.125 to 0.125
- norm_gain: float32 [2048], replicated, may hold values from 0.1 to 1.9
- gate_weight: bfloat16 [2048, 5632], P('sp', 'tp'), may hold values from -0.125 to 0.125
- up_weight: bfloat16 [2048, 5632], P('sp', 'tp'), may hold values from -0.125 to 0.125
- down_weight: bfloat16 [5632, 2048], P('tp', 'sp'), may hold values from -0.078125 to 0.078125
Outputs:
- mixed: bfloat16 [3072, 2048], P(('sp', 'tp'))
Inputs may be any that keep to these rules, and one draw needn't show every extreme that they name: `q_gain`: positive gains. `k_gain`: positive gains.
All inputs are finite; a program needn't handle non-finite values.
Results may differ from a plain program's by a relative error of at most 0.012.
The roundings to bfloat16 on the way count: a program that leaves them out, or rounds other values in their place, can miss the bound.
Values may be sent and summed in bfloat16 or wider, within the bound.
A program may use at most 128 MiB of HBM per device.

v0:
```python
import jax
import jax.numpy as jnp
from jax import lax
from jax.sharding import PartitionSpec as P

GRID_W = 64
EPSILON = 1e-06


def rotate(values, positions):
    dim_size = values.shape[-1]
    half_dim = dim_size // 2
    quarter = half_dim // 2
    inverse = 10000.0 ** (-jnp.arange(quarter, dtype=jnp.float32) / quarter)
    outputs = []
    for axis_pos, coords in enumerate((positions // GRID_W, positions % GRID_W)):
        angles = coords.astype(jnp.float32)[:, None] * inverse[None, :]
        cosine = jnp.cos(angles)[:, None, :]
        sine = jnp.sin(angles)[:, None, :]
        section = values[..., axis_pos * half_dim : (axis_pos + 1) * half_dim]
        first_half = section[..., :quarter]
        second_half = section[..., quarter:]
        outputs += [
            first_half * cosine - second_half * sine,
            second_half * cosine + first_half * sine,
        ]
    return jnp.concatenate(outputs, axis=-1)


def prepare(projected, gain, positions):
    values = projected.astype(jnp.float32)
    normed = values * lax.rsqrt(jnp.mean(values * values, axis=-1, keepdims=True) + EPSILON) * gain
    return rotate(normed, positions).astype(jnp.bfloat16)


def normalize(stream, gain):
    values = stream.astype(jnp.float32)
    return (
        values * lax.rsqrt(jnp.mean(values * values, axis=-1, keepdims=True) + EPSILON) * gain
    ).astype(jnp.bfloat16)


def body(
    resid,
    query,
    key,
    value,
    q_gain,
    k_gain,
    out_weight,
    norm_gain,
    gate_weight,
    up_weight,
    down_weight,
):
    rows_here = query.shape[0]
    head_dim = q_gain.shape[0]
    heads_here = query.shape[1] // head_dim
    kv_here = key.shape[1] // head_dim
    group_size = heads_here // kv_here
    score_scale = head_dim ** (-0.5)
    positions = lax.axis_index("sp") * rows_here + jnp.arange(rows_here, dtype=jnp.int32)
    q_rot = prepare(query.reshape(rows_here, heads_here, head_dim), q_gain, positions)
    k_rot = prepare(key.reshape(rows_here, kv_here, head_dim), k_gain, positions)
    val_rows = value.reshape(rows_here, kv_here, head_dim)
    grouped = q_rot.reshape(rows_here, kv_here, group_size, head_dim)

    def key_block(carry, block):
        maxima, totals, accum = carry
        block_keys, block_vals = block
        scores = (
            jnp.einsum("qkgd,skd->kgqs", grouped, block_keys, preferred_element_type=jnp.float32)
            * score_scale
        )
        new_max = jnp.maximum(maxima, jnp.max(scores, axis=-1))
        shrink = jnp.exp(maxima - new_max)
        weights = jnp.exp(scores - new_max[..., None])
        totals = totals * shrink + jnp.sum(weights, axis=-1)
        accum = accum * shrink[..., None] + jnp.einsum(
            "kgqs,skd->kgqd",
            weights.astype(jnp.bfloat16),
            block_vals,
            preferred_element_type=jnp.float32,
        )
        return ((new_max, totals, accum), None)

    start_max = jnp.full((kv_here, group_size, rows_here), -1e30, jnp.float32)
    start_total = jnp.zeros((kv_here, group_size, rows_here), jnp.float32)
    start_accum = jnp.zeros((kv_here, group_size, rows_here, head_dim), jnp.float32)
    carry = (start_max, start_total, start_accum)
    key_part = lax.all_gather(k_rot, "sp", axis=0, tiled=True)
    val_part = lax.all_gather(val_rows, "sp", axis=0, tiled=True)
    length = key_part.shape[0]
    factor = 4
    span = rows_here * factor
    turns = length // span
    key_blocks = key_part.reshape(turns, span, kv_here, head_dim)
    val_blocks = val_part.reshape(turns, span, kv_here, head_dim)
    carry, _ = lax.scan(key_block, carry, (key_blocks, val_blocks))
    maxima, totals, accum = carry
    attn = (
        jnp.transpose(accum / totals[..., None], (2, 0, 1, 3))
        .reshape(rows_here, heads_here * head_dim)
        .astype(jnp.bfloat16)
    )
    share = rows_here // lax.axis_size("tp")
    my_first = lax.axis_index("tp") * share
    proj = lax.psum_scatter(
        jnp.dot(attn, out_weight, preferred_element_type=jnp.float32).astype(jnp.bfloat16),
        "tp",
        scatter_dimension=0,
        tiled=True,
    ).astype(jnp.float32)
    my_resid = lax.dynamic_slice_in_dim(resid, my_first, share, 0)
    my_stream = (my_resid.astype(jnp.float32) + proj).astype(jnp.bfloat16)
    mixer_rows = lax.all_gather(normalize(my_stream, norm_gain), "tp", axis=0, tiled=True)

    def add_rows(shard_rows):
        return jnp.dot(mixer_rows, shard_rows, preferred_element_type=jnp.float32)

    gate = add_rows(lax.all_gather(gate_weight, "sp", axis=0, tiled=True))
    up_part = add_rows(lax.all_gather(up_weight, "sp", axis=0, tiled=True))
    hidden = (jax.nn.silu(gate) * up_part).astype(jnp.bfloat16)
    down_whole = lax.all_gather(down_weight, "sp", axis=1, tiled=True)
    down = lax.psum_scatter(
        jnp.dot(hidden, down_whole, preferred_element_type=jnp.float32).astype(jnp.bfloat16),
        "tp",
        scatter_dimension=0,
        tiled=True,
    ).astype(jnp.float32)
    return (my_stream.astype(jnp.float32) + 0.5 * down).astype(jnp.bfloat16)


def solution(mesh):
    placed = (
        P("sp", None),
        P("sp", "tp"),
        P("sp", "tp"),
        P("sp", "tp"),
        P(),
        P(),
        P("tp", None),
        P(),
        P("sp", "tp"),
        P("sp", "tp"),
        P("tp", "sp"),
    )
    return jax.shard_map(
        body, mesh=mesh, in_specs=placed, out_specs=P(("sp", "tp"), None), check_vma=False
    )
```

profile of v0, /device:TPU:0, one launch (start us, length us, event | category | flops | bytes accessed | tf_op | source)
XLA Modules:
  0.0 702.4 jit_solution(25329568361684075)
XLA Ops:
  6.6 1.1 reshape.193
  7.7 0.3 multiply_reduce_fusion.1
  8.0 0.9 multiply_multiply_fusion.1
  8.9 0.8 multiply_cosine_fusion.1
  9.7 0.7 subtract_convert_fusion.3
  10.4 1.3 pad_maximum_fusion.1
  11.7 0.0 all-gather.8.cloned.1.call-start
  11.8 0.7 reshape.191
  12.5 0.0 reduce-scatter.3.cloned.1.call-start
  12.6 0.1 convert_bitcast_fusion
  12.7 0.1 copy.65
  12.9 0.3 multiply_reduce_fusion
  13.1 0.1 copy.47
  13.2 0.1 copy.48
  13.4 0.3 multiply_multiply_fusion
  13.6 0.7 subtract_convert_fusion.1
  14.4 0.1 copy.49
  14.4 0.1 copy.50
  14.5 0.1 copy.51
  14.5 0.1 copy.52
  14.6 0.5 pad_maximum_fusion
  15.1 67.4 %all-gather.6.cloned.1.call-done = bf16[3072,4,128]{2,1,0:T(4,128)(2,1)} async-done(((bf16[192,4,128]{2,1,0:T(4,128)(2,1)}), bf16[3072,4,128]{2,1,0:T(4,128)(2,1)}) %all-gather.6.cloned.1.call-update) | async-done | bytes 3145744 | tf_op jit(solution)/shard_map/all_gather | solution.py:91
  82.5 69.2 %all-gather.8.cloned.1.call-done = bf16[3072,4,128]{2,1,0:T(4,128)(2,1)} async-done(((bf16[192,4,128]{2,1,0:T(4,128)(2,1)}), bf16[3072,4,128]{2,1,0:T(4,128)(2,1)}) %all-gather.8.cloned.1.call-update) | async-done | bytes 3145744 | tf_op jit(solution)/shard_map/all_gather | solution.py:92
  151.7 40.1 %while.15 = (s32[]{:T(128)}, f32[4,2,192]{2,1,0:T(2,128)S(1)}, f32[4,2,192]{2,1,0:T(2,128)S(1)}, f32[4,2,192,128]{3,2,1,0:T(8,128)S(1)}, bf16[4,768,4,128]{3,2,1...) while((s32[]{:T(128)}, f32[4,2,192]{2,1,0:T(2,128)S(1)}, ...), condition=%wide.region_5.6_spmd.clone, body=%wide.region_2.5_spmd.clone.sunk | while | flops 614014464 | bytes 39813256 | solution.py:99
  151.7 1.9 constant_dynamic-slice_fusion.3
  153.6 2.9 bitcast_reduce_fusion.2
  156.5 3.5 fusion.42
  160.1 0.2 copy-done
  160.3 1.4 fusion.44
  161.7 1.9 constant_dynamic-slice_fusion.3
  163.6 2.9 bitcast_reduce_fusion.2
  166.6 3.5 fusion.42
  170.1 0.2 copy-done
  170.3 1.4 fusion.44
  171.7 1.9 constant_dynamic-slice_fusion.3
  173.6 2.9 bitcast_reduce_fusion.2
  176.6 3.5 fusion.42
  180.1 0.2 copy-done
  180.3 1.4 fusion.44
  181.7 1.9 constant_dynamic-slice_fusion.3
  183.7 2.9 bitcast_reduce_fusion.2
  186.6 3.5 fusion.42
  190.2 0.2 copy-done
  190.3 1.4 fusion.44
  191.8 0.3 fusion.19
  192.0 0.4 copy.56
  192.5 0.3 convert_element_type.83
  192.8 4.1 convolution_convert_fusion.1
  196.9 0.0 all-gather.10.cloned.1.call-start
  196.9 0.5 all-gather.10.cloned.1.call-update
  197.5 0.5 all-gather.12.cloned.1.call-update
  198.1 0.5 all-gather.14.cloned.1.call-update
  198.6 0.0 reduce-scatter.5.cloned.1.call-start
  198.7 5.1 reduce-scatter.3.cloned.1.call-done
  203.8 1.2 fusion.15
  205.0 0.2 fusion.17
  205.2 2.5 all_gather.20
  207.7 141.2 %all-gather.10.cloned.1.call-done = bf16[2048,2816]{1,0:T(8,128)(2,1)} async-done(((bf16[128,2816]{1,0:T(8,128)(2,1)}), bf16[2048,2816]{1,0:T(8,128)(2,1)}) %all-gather.10.cloned.1.call-update) | async-done | bytes 11534352 | tf_op jit(solution)/shard_map/all_gather | solution.py:121
  348.9 6.7 fusion.24
  355.6 135.6 %all-gather.12.cloned.1.call-done = bf16[2048,2816]{1,0:T(8,128)(2,1)} async-done(((bf16[128,2816]{1,0:T(8,128)(2,1)}), bf16[2048,2816]{1,0:T(8,128)(2,1)}) %all-gather.12.cloned.1.call-update) | async-done | bytes 11534352 | tf_op jit(solution)/shard_map/all_gather | solution.py:122
  491.2 182.8 %all-gather.14.cloned.1.call-done = bf16[2816,2048]{1,0:T(8,128)(2,1)} async-done(((bf16[2816,128]{1,0:T(8,128)(2,1)}), bf16[2816,2048]{1,0:T(8,128)(2,1)}) %all-gather.14.cloned.1.call-update) | async-done | bytes 11534352 | tf_op jit(solution)/shard_map/all_gather | solution.py:124
  674.0 13.2 %convolution_convert_fusion = bf16[192,2048]{1,0:T(8,128)(2,1)} fusion(bf16[2816,2048]{1,0:T(8,128)(2,1)} %all-gather.14.cloned.1.call-done, bf16[192,2048]{1,0:T(8,128)(2,1)S(1)} %all_gather.20, bf16[2048,2816]{1,0:T(8,128)(2,1)} %all-gather.12.cloned.1.call-done, f32[192,2816]{1,0:T(8,128)S(1)} %fusion.24), kind=kOutput, calls=%fused_computation.23 | convolution fusion | flops 4432822272 | bytes 26804224 | tf_op jit(solution)/shard_map/dot_general | solution.py:126
  687.2 6.5 reduce-scatter.5.cloned.1.call-done
  693.7 1.9 fusion.18
  (41 shorter events, 0.4 us)
Async XLA Ops:
  6.5 5.2 copy-start.2
  6.5 6.1 copy-start.1
  6.5 75.9 %all-gather.6.cloned.1.call-start = ((), (), s32[]{:S(2)}) async-start(), calls=%async_computation.2 | async-start | bytes 3342336 | tf_op jit(solution)/shard_map/all_gather | solution.py:91
  8.0 5.3 copy-start.5
  11.7 140.0 %all-gather.8.cloned.1.call-start = ((), (), s32[]{:S(2)}) async-start(), calls=%async_computation.3 | async-start | bytes 3342336 | tf_op jit(solution)/shard_map/all_gather | solution.py:92
  12.5 191.2 %reduce-scatter.3.cloned.1.call-start = ((), (), s32[]{:S(2)}) async-start(), calls=%async_computation.4 | async-start | bytes 1179648 | tf_op jit(solution)/shard_map/reduce_scatter | solution.py:108
  156.5 3.8 copy-start
  166.5 3.8 copy-start
  176.6 3.8 copy-start
  186.6 3.8 copy-start
  192.5 11.3 %copy-start.3 = (bf16[192,2048]{1,0:T(8,128)(2,1)S(1)}, bf16[192,2048]{1,0:T(8,128)(2,1)}, u32[]{:S(2)}) copy-start(bf16[192,2048]{1,0:T(8,128)(2,1)} %param.13) | copy-start | bytes 2359300
  192.7 12.3 %copy-start.4 = (f32[2048]{0:T(1024)S(1)}, f32[2048]{0:T(1024)}, u32[]{:S(2)}) copy-start(f32[2048]{0:T(1024)} %param.20) | copy-start | bytes 24580
  196.9 152.0 %all-gather.10.cloned.1.call-start = ((), (), s32[]{:S(2)}) async-start(), calls=%async_computation.5 | async-start | bytes 12255232 | tf_op jit(solution)/shard_map/all_gather | solution.py:121
  197.5 293.7 %all-gather.12.cloned.1.call-start = ((), (), s32[]{:S(2)}) async-start(), calls=%async_computation.6 | async-start | bytes 12255232 | tf_op jit(solution)/shard_map/all_gather | solution.py:122
  198.1 475.9 %all-gather.14.cloned.1.call-start = ((), (), s32[]{:S(2)}) async-start(), calls=%async_computation.7 | async-start | bytes 12255232 | tf_op jit(solution)/shard_map/all_gather | solution.py:124
  198.6 495.1 %reduce-scatter.5.cloned.1.call-start = ((), (), s32[]{:S(2)}) async-start(), calls=%async_computation.8 | async-start | bytes 1179648 | tf_op jit(solution)/shard_map/reduce_scatter | solution.py:125
Sparse Core Ops, SparseCore 0:
  11.9 70.5 all-gather.5
  85.2 66.3 all-gather.7
  197.0 6.6 reduce-scatter.2
  206.4 142.5 all-gather.9
  351.5 139.5 all-gather.11
  493.7 180.2 all-gather.13
  687.3 6.3 reduce-scatter.4
where the time goes:
time: 703 us; the launch traced here: 702 us
  waiting for transfers between devices  609 us (87%)
  matrix products  41.2 us (6%)
  other arithmetic  23.7 us (3%)
  between operations  13.8 us (2%)
  local copies, waits for them, and re-layouts  11.4 us (2%)
    all_gather x1, waiting for transfers between devices, body(): down_whole = lax.all_gather(down_weight, 'sp', axis=1, tiled=True)  183 us
    all_gather x1, waiting for transfers between devices, body(): gate = add_rows(lax.all_gather(gate_weight, 'sp', axis=0, tiled=True))  141 us
    all_gather x1, waiting for transfers between devices, body(): up_part = add_rows(lax.all_gather(up_weight, 'sp', axis=0, tiled=True))  136 us
    all_gather x1, waiting for transfers between devices, body(): val_part = lax.all_gather(val_rows, 'sp', axis=0, tiled=True)  69.2 us
    all_gather x1, waiting for transfers between devices, body(): key_part = lax.all_gather(k_rot, 'sp', axis=0, tiled=True)  67.4 us
    reduce_sum x4, other arithmetic, key_block(): totals = totals * shrink + jnp.sum(weights, axis=-1)  14.2 us
  transfers between devices with their start and end apart: 7, of which 7 were waited for; matrix products, arithmetic and copies ran while one was open for 2% of the time, Pallas kernels for 0%

commit v1 on v0

--- a/solution.py
+++ b/solution.py
@@ -5,6 +5,18 @@
 
 GRID_W = 64
 EPSILON = 1e-06
+
+
+def meshes_begin(u_in):
+    num_devices = lax.axis_size("sp")
+    odd = u_in
+    leaves = [odd]
+    taken_in = [(no - 1, no) for no in range(1, num_devices)] + [(num_devices - 1, 0)]
+    for _ in [*range(num_devices - 1)]:
+        odd = lax.ppermute(odd, "sp", taken_in)
+        leaves += [odd]
+    small = jnp.concatenate([*reversed(leaves)], axis=0)
+    return jnp.roll(small, (lax.axis_index("sp") + 1) * odd.shape[0], axis=0)
 
 
 def rotate(values, positions):
@@ -88,7 +100,7 @@
     start_total = jnp.zeros((kv_here, group_size, rows_here), jnp.float32)
     start_accum = jnp.zeros((kv_here, group_size, rows_here, head_dim), jnp.float32)
     carry = (start_max, start_total, start_accum)
-    key_part = lax.all_gather(k_rot, "sp", axis=0, tiled=True)
+    key_part = meshes_begin(k_rot)
     val_part = lax.all_gather(val_rows, "sp", axis=0, tiled=True)
     length = key_part.shape[0]
     factor = 4

time: 703 us -> 751 us (1.068)
  local copies, waits for them, and re-layouts: 11.4 us -> 35 us
  waiting for transfers between devices: 609 us -> 624 us
    ppermute x0 -> x15, waiting for transfers between devices: none -> 154 us  [meshes_begin(): odd = lax.ppermute(odd, 'sp', taken_in)]
    all_gather x1, waiting for transfers between devices: 69.2 us -> 0.01 us  [body(): val_part = lax.all_gather(val_rows, 'sp', axis=0, tiled=True)]
    all_gather x1 -> x0, waiting for transfers between devices: 67.4 us -> none  [body(): key_part = lax.all_gather(k_rot, 'sp', axis=0, tiled=True)]
    unnamed x11 -> x68, local copies, waits for them, and re-layouts: 0.17 us -> 21.5 us
  transfers between devices with their start and end apart: 7 -> 21, of which waited for: 7 -> 20; matrix products, arithmetic and copies ran while one was open for 2% -> 5% of each run, Pallas kernels for 0% -> 0%
where the time goes in v1:
time: 751 us; the launch traced here: 750 us
  waiting for transfers between devices  624 us (83%)
  matrix products  48 us (6%)
  local copies, waits for them, and re-layouts  35 us (5%)
  other arithmetic  22.4 us (3%)
  between operations  13.9 us (2%)
    all_gather x1, waiting for transfers between devices, body(): down_whole = lax.all_gather(down_weight, 'sp', axis=1, tiled=True)  176 us
    ppermute x15, waiting for transfers between devices, meshes_begin(): odd = lax.ppermute(odd, 'sp', taken_in)  154 us
    all_gather x1, waiting for transfers between devices, body(): up_part = add_rows(lax.all_gather(up_weight, 'sp', axis=0, tiled=True))  142 us
    all_gather x1, waiting for transfers between devices, body(): gate = add_rows(lax.all_gather(gate_weight, 'sp', axis=0, tiled=True))  141 us
    unnamed x68, local copies, waits for them, and re-layouts  21.5 us
  transfers between devices with their start and end apart: 21, of which 20 were waited for; matrix products, arithmetic and copies ran while one was open for 5% of the time, Pallas kernels for 0%

profile of v1, /device:TPU:0, one launch (start us, length us, event | category | flops | bytes accessed | tf_op | source)
XLA Modules:
  0.0 749.6 jit_solution(13346388711540857105)
XLA Ops:
  6.6 1.1 reshape.193
  11.0 3.0 collective-permute-start
  14.0 8.9 %collective-permute-done = bf16[192,4,128]{2,1,0:T(4,128)(2,1)S(1)} collective-permute-done((bf16[192,4,128]{2,1,0:T(4,128)(2,1)S(1)}, bf16[192,4,128]{2,1,0:T(4,128)(2,1)S(1)}, u32[]{:S(2)}, u32[]{:S(2)}) %collective-permute-start) | collective-permute-done | bytes 196640 | tf_op jit(solution)/shard_map/ppermute | solution.py:16
  22.9 9.7 %collective-permute-done.1 = bf16[192,4,128]{2,1,0:T(4,128)(2,1)S(1)} collective-permute-done((bf16[192,4,128]{2,1,0:T(4,128)(2,1)S(1)}, bf16[192,4,128]{2,1,0:T(4,128)(2,1)S(1)}, u32[]{:S(2)}, u32[]{:S(2)}) %collective-permute-start.1) | collective-permute-done | bytes 196640 | tf_op jit(solution)/shard_map/ppermute | solution.py:16
  32.6 9.3 %collective-permute-done.2 = bf16[192,4,128]{2,1,0:T(4,128)(2,1)S(1)} collective-permute-done((bf16[192,4,128]{2,1,0:T(4,128)(2,1)S(1)}, bf16[192,4,128]{2,1,0:T(4,128)(2,1)S(1)}, u32[]{:S(2)}, u32[]{:S(2)}) %collective-permute-start.2) | collective-permute-done | bytes 196640 | tf_op jit(solution)/shard_map/ppermute | solution.py:16
  41.9 9.3 %collective-permute-done.3 = bf16[192,4,128]{2,1,0:T(4,128)(2,1)S(1)} collective-permute-done((bf16[192,4,128]{2,1,0:T(4,128)(2,1)S(1)}, bf16[192,4,128]{2,1,0:T(4,128)(2,1)S(1)}, u32[]{:S(2)}, u32[]{:S(2)}) %collective-permute-start.3) | collective-permute-done | bytes 196640 | tf_op jit(solution)/shard_map/ppermute | solution.py:16
  51.1 9.3 %collective-permute-done.4 = bf16[192,4,128]{2,1,0:T(4,128)(2,1)S(1)} collective-permute-done((bf16[192,4,128]{2,1,0:T(4,128)(2,1)S(1)}, bf16[192,4,128]{2,1,0:T(4,128)(2,1)S(1)}, u32[]{:S(2)}, u32[]{:S(2)}) %collective-permute-start.4) | collective-permute-done | bytes 196640 | tf_op jit(solution)/shard_map/ppermute | solution.py:16
  60.4 9.3 %collective-permute-done.5 = bf16[192,4,128]{2,1,0:T(4,128)(2,1)S(1)} collective-permute-done((bf16[192,4,128]{2,1,0:T(4,128)(2,1)S(1)}, bf16[192,4,128]{2,1,0:T(4,128)(2,1)S(1)}, u32[]{:S(2)}, u32[]{:S(2)}) %collective-permute-start.5) | collective-permute-done | bytes 196640 | tf_op jit(solution)/shard_map/ppermute | solution.py:16
  69.7 10.4 %collective-permute-done.6 = bf16[192,4,128]{2,1,0:T(4,128)(2,1)S(1)} collective-permute-done((bf16[192,4,128]{2,1,0:T(4,128)(2,1)S(1)}, bf16[192,4,128]{2,1,0:T(4,128)(2,1)S(1)}, u32[]{:S(2)}, u32[]{:S(2)}) %collective-permute-start.6) | collective-permute-done | bytes 196640 | tf_op jit(solution)/shard_map/ppermute | solution.py:16
  80.9 10.3 %collective-permute-done.7 = bf16[192,4,128]{2,1,0:T(4,128)(2,1)S(1)} collective-permute-done((bf16[192,4,128]{2,1,0:T(4,128)(2,1)S(1)}, bf16[192,4,128]{2,1,0:T(4,128)(2,1)S(1)}, u32[]{:S(2)}, u32[]{:S(2)}) %collective-permute-start.7) | collective-permute-done | bytes 196640 | tf_op jit(solution)/shard_map/ppermute | solution.py:16
  91.3 14.1 %collective-permute-done.8 = bf16[192,4,128]{2,1,0:T(4,128)(2,1)S(1)} collective-permute-done((bf16[192,4,128]{2,1,0:T(4,128)(2,1)S(1)}, bf16[192,4,128]{2,1,0:T(4,128)(2,1)S(1)}, u32[]{:S(2)}, u32[]{:S(2)}) %collective-permute-start.8) | collective-permute-done | bytes 196640 | tf_op jit(solution)/shard_map/ppermute | solution.py:16
  105.4 10.2 %collective-permute-done.9 = bf16[192,4,128]{2,1,0:T(4,128)(2,1)S(1)} collective-permute-done((bf16[192,4,128]{2,1,0:T(4,128)(2,1)S(1)}, bf16[192,4,128]{2,1,0:T(4,128)(2,1)S(1)}, u32[]{:S(2)}, u32[]{:S(2)}) %collective-permute-start.9) | collective-permute-done | bytes 196640 | tf_op jit(solution)/shard_map/ppermute | solution.py:16
  115.6 10.2 %collective-permute-done.10 = bf16[192,4,128]{2,1,0:T(4,128)(2,1)S(1)} collective-permute-done((bf16[192,4,128]{2,1,0:T(4,128)(2,1)S(1)}, bf16[192,4,128]{2,1,0:T(4,128)(2,1)S(1)}, u32[]{:S(2)}, u32[]{:S(2)}) %collective-permute-start.10) | collective-permute-done | bytes 196640 | tf_op jit(solution)/shard_map/ppermute | solution.py:16
  126.4 8.7 %collective-permute-done.11 = bf16[192,4,128]{2,1,0:T(4,128)(2,1)S(1)} collective-permute-done((bf16[192,4,128]{2,1,0:T(4,128)(2,1)S(1)}, bf16[192,4,128]{2,1,0:T(4,128)(2,1)S(1)}, u32[]{:S(2)}, u32[]{:S(2)}) %collective-permute-start.11) | collective-permute-done | bytes 196640 | tf_op jit(solution)/shard_map/ppermute | solution.py:16
  135.2 13.5 %collective-permute-done.12 = bf16[192,4,128]{2,1,0:T(4,128)(2,1)S(1)} collective-permute-done((bf16[192,4,128]{2,1,0:T(4,128)(2,1)S(1)}, bf16[192,4,128]{2,1,0:T(4,128)(2,1)S(1)}, u32[]{:S(2)}, u32[]{:S(2)}) %collective-permute-start.12) | collective-permute-done | bytes 196640 | tf_op jit(solution)/shard_map/ppermute | solution.py:16
  149.0 12.9 %collective-permute-done.13 = bf16[192,4,128]{2,1,0:T(4,128)(2,1)} collective-permute-done((bf16[192,4,128]{2,1,0:T(4,128)(2,1)S(1)}, bf16[192,4,128]{2,1,0:T(4,128)(2,1)}, u32[]{:S(2)}, u32[]{:S(2)}) %collective-permute-start.13) | collective-permute-done | bytes 196640 | tf_op jit(solution)/shard_map/ppermute | solution.py:16
  163.8 7.9 %collective-permute-done.14 = bf16[192,4,128]{2,1,0:T(4,128)(2,1)} collective-permute-done((bf16[192,4,128]{2,1,0:T(4,128)(2,1)}, bf16[192,4,128]{2,1,0:T(4,128)(2,1)}, u32[]{:S(2)}, u32[]{:S(2)}) %collective-permute-start.14) | collective-permute-done | bytes 196640 | tf_op jit(solution)/shard_map/ppermute | solution.py:16
  172.7 1.0 constant_dynamic-update-slice_fusion.30
  173.7 1.0 constant_dynamic-update-slice_fusion.29
  174.8 1.0 constant_dynamic-update-slice_fusion.28
  175.8 1.0 constant_dynamic-update-slice_fusion.27
  176.8 1.0 constant_dynamic-update-slice_fusion.26
  177.8 1.0 constant_dynamic-update-slice_fusion.25
  178.8 1.0 constant_dynamic-update-slice_fusion.24
  179.8 1.0 constant_dynamic-update-slice_fusion.23
  180.9 1.0 constant_dynamic-update-slice_fusion.22
  181.9 1.0 constant_dynamic-update-slice_fusion.21
  183.4 1.0 constant_dynamic-update-slice_fusion.15
  184.4 1.0 constant_dynamic-update-slice_fusion.14
  185.5 1.0 constant_dynamic-update-slice_fusion.12
  186.5 1.0 constant_dynamic-update-slice_fusion.11
  187.5 1.0 constant_dynamic-update-slice_fusion.10
  188.5 1.0 constant_dynamic-update-slice_fusion.9
  189.6 1.0 constant_dynamic-update-slice_fusion.8
  191.6 1.0 constant_dynamic-update-slice_fusion.6
  193.2 2.8 constant_dynamic-slice_fusion.2
  195.9 45.6 %while.15 = (s32[]{:T(128)}, f32[4,2,192]{2,1,0:T(2,128)S(1)}, f32[4,2,192]{2,1,0:T(2,128)S(1)}, f32[4,2,192,128]{3,2,1,0:T(8,128)S(1)}, bf16[4,768,4,128]{3,2,1...) while((s32[]{:T(128)}, f32[4,2,192]{2,1,0:T(2,128)S(1)}, ...), condition=%wide.region_5.6_spmd.clone, body=%wide.region_2.5_spmd.clone.sunk | while | flops 614014464 | bytes 20938860 | solution.py:111
  195.9 1.9 constant_dynamic-slice_fusion.4
  197.9 2.9 bitcast_reduce_fusion.2
  200.8 3.4 fusion.42
  204.2 3.1 fusion.44
  207.4 1.9 constant_dynamic-slice_fusion.4
  209.3 2.9 bitcast_reduce_fusion.2
  212.2 3.4 fusion.42
  215.6 3.1 fusion.44
  218.8 1.9 constant_dynamic-slice_fusion.4
  220.7 2.9 bitcast_reduce_fusion.2
  223.6 3.4 fusion.42
  227.0 3.1 fusion.44
  230.2 1.9 constant_dynamic-slice_fusion.4
  232.1 2.9 bitcast_reduce_fusion.2
  235.0 3.4 fusion.42
  238.5 3.1 fusion.44
  242.6 4.1 convolution_convert_fusion.1
  248.6 2.2 reduce-scatter.3.cloned.1.call-done
  250.8 1.2 fusion.15
  252.3 2.6 all_gather.16
  254.9 141.3 %all-gather.7.cloned.1.call-done = bf16[2048,2816]{1,0:T(8,128)(2,1)} async-done(((bf16[128,2816]{1,0:T(8,128)(2,1)}), bf16[2048,2816]{1,0:T(8,128)(2,1)}) %all-gather.7.cloned.1.call-update) | async-done | bytes 11534352 | tf_op jit(solution)/shard_map/all_gather | solution.py:133
  396.2 6.7 fusion.24
  402.9 176.1 %all-gather.11.cloned.1.call-done = bf16[2816,2048]{1,0:T(8,128)(2,1)} async-done(((bf16[2816,128]{1,0:T(8,128)(2,1)}), bf16[2816,2048]{1,0:T(8,128)(2,1)}) %all-gather.11.cloned.1.call-update) | async-done | bytes 11534352 | tf_op jit(solution)/shard_map/all_gather | solution.py:136
  579.0 142.2 %all-gather.9.cloned.1.call-done = bf16[2048,2816]{1,0:T(8,128)(2,1)} async-done(((bf16[128,2816]{1,0:T(8,128)(2,1)}), bf16[2048,2816]{1,0:T(8,128)(2,1)}) %all-gather.9.cloned.1.call-update) | async-done | bytes 11534352 | tf_op jit(solution)/shard_map/all_gather | solution.py:134
  721.2 13.2 %convolution_convert_fusion = bf16[192,2048]{1,0:T(8,128)(2,1)} fusion(bf16[2816,2048]{1,0:T(8,128)(2,1)} %all-gather.11.cloned.1.call-done, bf16[192,2048]{1,0:T(8,128)(2,1)S(1)} %all_gather.16, bf16[2048,2816]{1,0:T(8,128)(2,1)} %all-gather.9.cloned.1.call-done, f32[192,2816]{1,0:T(8,128)S(1)} %fusion.24), kind=kOutput, calls=%fused_computation.23 | convolution fusion | flops 4432822272 | bytes 26804224 | tf_op jit(solution)/shard_map/dot_general | solution.py:138
  734.4 6.5 reduce-scatter.5.cloned.1.call-done
  740.9 1.9 fusion.18
  (119 shorter events, 13.2 us)
Async XLA Ops:
  6.5 73.6 %copy-start.14 = (bf16[192,512]{1,0:T(8,128)(2,1)S(1)}, bf16[192,512]{1,0:T(8,128)(2,1)}, u32[]{:S(2)}) copy-start(bf16[192,512]{1,0:T(8,128)(2,1)} %param.16) | copy-start | bytes 589828
  6.5 119.2 %copy-start.13 = (bf16[192,1024]{1,0:T(8,128)(2,1)S(1)}, bf16[192,1024]{1,0:T(8,128)(2,1)}, u32[]{:S(2)}) copy-start(bf16[192,1024]{1,0:T(8,128)(2,1)} %param.14) | copy-start | bytes 1179652
  6.5 142.2 %copy-start.17 = (f32[128]{0:T(128)S(1)}, f32[128]{0:T(128)}, u32[]{:S(2)}) copy-start(f32[128]{0:T(128)} %param.17) | copy-start | bytes 1540
  6.5 189.4 %all-gather.5.cloned.1.call-start = ((), (), s32[]{:S(2)}) async-start(), calls=%async_computation.2 | async-start | bytes 3342336 | tf_op jit(solution)/shard_map/all_gather | solution.py:104
  11.0 11.9 %collective-permute-start = (bf16[192,4,128]{2,1,0:T(4,128)(2,1)S(1)}, bf16[192,4,128]{2,1,0:T(4,128)(2,1)S(1)}, u32[]{:S(2)}, u32[]{:S(2)}) collective-permute-start(bf16[192,4,128]{2,1,0:T(4,128)(2,1)S(1)} %pad_maximum_fusion.1), channel_id=1, source_target_pairs={{0,2},{2,4},{4,6},{6,8},{8,10},{10,12},{12,14},{14,16},{16,18},{18... | collective-permute-start | bytes 589832 | tf_op jit(solution)/shard_map/ppermute | solution.py:16
  22.9 9.7 %collective-permute-start.1 = (bf16[192,4,128]{2,1,0:T(4,128)(2,1)S(1)}, bf16[192,4,128]{2,1,0:T(4,128)(2,1)S(1)}, u32[]{:S(2)}, u32[]{:S(2)}) collective-permute-start(bf16[192,4,128]{2,1,0:T(4,128)(2,1)S(1)} %collective-permute-done), channel_id=1, source_target_pairs={{0,2},{2,4},{4,6},{6,8},{8,10},{10,12},{12,14},{14,16},{16,18},{18... | collective-permute-start | bytes 589832 | tf_op jit(solution)/shard_map/ppermute | solution.py:16
  32.6 9.3 %collective-permute-start.2 = (bf16[192,4,128]{2,1,0:T(4,128)(2,1)S(1)}, bf16[192,4,128]{2,1,0:T(4,128)(2,1)S(1)}, u32[]{:S(2)}, u32[]{:S(2)}) collective-permute-start(bf16[192,4,128]{2,1,0:T(4,128)(2,1)S(1)} %collective-permute-done.1), channel_id=1, source_target_pairs={{0,2},{2,4},{4,6},{6,8},{8,10},{10,12},{12,14},{14,16},{16,18},{18... | collective-permute-start | bytes 589832 | tf_op jit(solution)/shard_map/ppermute | solution.py:16
  41.9 9.3 %collective-permute-start.3 = (bf16[192,4,128]{2,1,0:T(4,128)(2,1)S(1)}, bf16[192,4,128]{2,1,0:T(4,128)(2,1)S(1)}, u32[]{:S(2)}, u32[]{:S(2)}) collective-permute-start(bf16[192,4,128]{2,1,0:T(4,128)(2,1)S(1)} %collective-permute-done.2), channel_id=1, source_target_pairs={{0,2},{2,4},{4,6},{6,8},{8,10},{10,12},{12,14},{14,16},{16,18},{18... | collective-permute-start | bytes 589832 | tf_op jit(solution)/shard_map/ppermute | solution.py:16
  51.1 110.8 %copy-start = (bf16[192,4,128]{2,1,0:T(4,128)(2,1)}, bf16[192,4,128]{2,1,0:T(4,128)(2,1)S(1)}, u32[]{:S(2)}) copy-start(bf16[192,4,128]{2,1,0:T(4,128)(2,1)S(1)} %collective-permute-done.3) | copy-start | bytes 589828
  51.1 9.3 %collective-permute-start.4 = (bf16[192,4,128]{2,1,0:T(4,128)(2,1)S(1)}, bf16[192,4,128]{2,1,0:T(4,128)(2,1)S(1)}, u32[]{:S(2)}, u32[]{:S(2)}) collective-permute-start(bf16[192,4,128]{2,1,0:T(4,128)(2,1)S(1)} %collective-permute-done.3), channel_id=1, source_target_pairs={{0,2},{2,4},{4,6},{6,8},{8,10},{10,12},{12,14},{14,16},{16,18},{18... | collective-permute-start | bytes 589832 | tf_op jit(solution)/shard_map/ppermute | solution.py:16
  60.4 101.5 %copy-start.2 = (bf16[192,4,128]{2,1,0:T(4,128)(2,1)}, bf16[192,4,128]{2,1,0:T(4,128)(2,1)S(1)}, u32[]{:S(2)}) copy-start(bf16[192,4,128]{2,1,0:T(4,128)(2,1)S(1)} %collective-permute-done.4) | copy-start | bytes 589828
  60.4 9.3 %collective-permute-start.5 = (bf16[192,4,128]{2,1,0:T(4,128)(2,1)S(1)}, bf16[192,4,128]{2,1,0:T(4,128)(2,1)S(1)}, u32[]{:S(2)}, u32[]{:S(2)}) collective-permute-start(bf16[192,4,128]{2,1,0:T(4,128)(2,1)S(1)} %collective-permute-done.4), channel_id=1, source_target_pairs={{0,2},{2,4},{4,6},{6,8},{8,10},{10,12},{12,14},{14,16},{16,18},{18... | collective-permute-start | bytes 589832 | tf_op jit(solution)/shard_map/ppermute | solution.py:16
  69.7 92.2 %copy-start.4 = (bf16[192,4,128]{2,1,0:T(4,128)(2,1)}, bf16[192,4,128]{2,1,0:T(4,128)(2,1)S(1)}, u32[]{:S(2)}) copy-start(bf16[192,4,128]{2,1,0:T(4,128)(2,1)S(1)} %collective-permute-done.5) | copy-start | bytes 589828
  69.7 10.4 %collective-permute-start.6 = (bf16[192,4,128]{2,1,0:T(4,128)(2,1)S(1)}, bf16[192,4,128]{2,1,0:T(4,128)(2,1)S(1)}, u32[]{:S(2)}, u32[]{:S(2)}) collective-permute-start(bf16[192,4,128]{2,1,0:T(4,128)(2,1)S(1)} %collective-permute-done.5), channel_id=1, source_target_pairs={{0,2},{2,4},{4,6},{6,8},{8,10},{10,12},{12,14},{14,16},{16,18},{18... | collective-permute-start | bytes 589832 | tf_op jit(solution)/shard_map/ppermute | solution.py:16
  80.1 81.8 %copy-start.5 = (bf16[192,4,128]{2,1,0:T(4,128)(2,1)}, bf16[192,4,128]{2,1,0:T(4,128)(2,1)S(1)}, u32[]{:S(2)}) copy-start(bf16[192,4,128]{2,1,0:T(4,128)(2,1)S(1)} %collective-permute-done.6) | copy-start | bytes 589828
  80.1 11.2 %collective-permute-start.7 = (bf16[192,4,128]{2,1,0:T(4,128)(2,1)S(1)}, bf16[192,4,128]{2,1,0:T(4,128)(2,1)S(1)}, u32[]{:S(2)}, u32[]{:S(2)}) collective-permute-start(bf16[192,4,128]{2,1,0:T(4,128)(2,1)S(1)} %collective-permute-done.6), channel_id=1, source_target_pairs={{0,2},{2,4},{4,6},{6,8},{8,10},{10,12},{12,14},{14,16},{16,18},{18... | collective-permute-start | bytes 589832 | tf_op jit(solution)/shard_map/ppermute | solution.py:16
  80.9 169.9 %reduce-scatter.3.cloned.1.call-start = ((), (), s32[]{:S(2)}) async-start(), calls=%async_computation.3 | async-start | bytes 1179648 | tf_op jit(solution)/shard_map/reduce_scatter | solution.py:120
  91.3 34.5 %copy-start.6 = (bf16[192,4,128]{2,1,0:T(4,128)(2,1)}, bf16[192,4,128]{2,1,0:T(4,128)(2,1)S(1)}, u32[]{:S(2)}) copy-start(bf16[192,4,128]{2,1,0:T(4,128)(2,1)S(1)} %collective-permute-done.7) | copy-start | bytes 589828
  91.3 14.1 %collective-permute-start.8 = (bf16[192,4,128]{2,1,0:T(4,128)(2,1)S(1)}, bf16[192,4,128]{2,1,0:T(4,128)(2,1)S(1)}, u32[]{:S(2)}, u32[]{:S(2)}) collective-permute-start(bf16[192,4,128]{2,1,0:T(4,128)(2,1)S(1)} %collective-permute-done.7), channel_id=1, source_target_pairs={{0,2},{2,4},{4,6},{6,8},{8,10},{10,12},{12,14},{14,16},{16,18},{18... | collective-permute-start | bytes 589832 | tf_op jit(solution)/shard_map/ppermute | solution.py:16
  105.4 20.4 %copy-start.7 = (bf16[192,4,128]{2,1,0:T(4,128)(2,1)}, bf16[192,4,128]{2,1,0:T(4,128)(2,1)S(1)}, u32[]{:S(2)}) copy-start(bf16[192,4,128]{2,1,0:T(4,128)(2,1)S(1)} %collective-permute-done.8) | copy-start | bytes 589828
  105.4 10.2 %collective-permute-start.9 = (bf16[192,4,128]{2,1,0:T(4,128)(2,1)S(1)}, bf16[192,4,128]{2,1,0:T(4,128)(2,1)S(1)}, u32[]{:S(2)}, u32[]{:S(2)}) collective-permute-start(bf16[192,4,128]{2,1,0:T(4,128)(2,1)S(1)} %collective-permute-done.8), channel_id=1, source_target_pairs={{0,2},{2,4},{4,6},{6,8},{8,10},{10,12},{12,14},{14,16},{16,18},{18... | collective-permute-start | bytes 589832 | tf_op jit(solution)/shard_map/ppermute | solution.py:16
  115.6 10.2 %copy-start.8 = (bf16[192,4,128]{2,1,0:T(4,128)(2,1)}, bf16[192,4,128]{2,1,0:T(4,128)(2,1)S(1)}, u32[]{:S(2)}) copy-start(bf16[192,4,128]{2,1,0:T(4,128)(2,1)S(1)} %collective-permute-done.9) | copy-start | bytes 589828
  115.6 10.2 %collective-permute-start.10 = (bf16[192,4,128]{2,1,0:T(4,128)(2,1)S(1)}, bf16[192,4,128]{2,1,0:T(4,128)(2,1)S(1)}, u32[]{:S(2)}, u32[]{:S(2)}) collective-permute-start(bf16[192,4,128]{2,1,0:T(4,128)(2,1)S(1)} %collective-permute-done.9), channel_id=1, source_target_pairs={{0,2},{2,4},{4,6},{6,8},{8,10},{10,12},{12,14},{14,16},{16,18},{18... | collective-permute-start | bytes 589832 | tf_op jit(solution)/shard_map/ppermute | solution.py:16
  125.7 37.2 %copy-start.9 = (bf16[192,4,128]{2,1,0:T(4,128)(2,1)}, bf16[192,4,128]{2,1,0:T(4,128)(2,1)S(1)}, u32[]{:S(2)}) copy-start(bf16[192,4,128]{2,1,0:T(4,128)(2,1)S(1)} %collective-permute-done.10) | copy-start | bytes 589828
  125.8 9.3 %collective-permute-start.11 = (bf16[192,4,128]{2,1,0:T(4,128)(2,1)S(1)}, bf16[192,4,128]{2,1,0:T(4,128)(2,1)S(1)}, u32[]{:S(2)}, u32[]{:S(2)}) collective-permute-start(bf16[192,4,128]{2,1,0:T(4,128)(2,1)S(1)} %collective-permute-done.10), channel_id=1, source_target_pairs={{0,2},{2,4},{4,6},{6,8},{8,10},{10,12},{12,14},{14,16},{16,18},{18... | collective-permute-start | bytes 589832 | tf_op jit(solution)/shard_map/ppermute | solution.py:16
  135.1 27.8 %copy-start.10 = (bf16[192,4,128]{2,1,0:T(4,128)(2,1)}, bf16[192,4,128]{2,1,0:T(4,128)(2,1)S(1)}, u32[]{:S(2)}) copy-start(bf16[192,4,128]{2,1,0:T(4,128)(2,1)S(1)} %collective-permute-done.11) | copy-start | bytes 589828
  135.1 13.6 %collective-permute-start.12 = (bf16[192,4,128]{2,1,0:T(4,128)(2,1)S(1)}, bf16[192,4,128]{2,1,0:T(4,128)(2,1)S(1)}, u32[]{:S(2)}, u32[]{:S(2)}) collective-permute-start(bf16[192,4,128]{2,1,0:T(4,128)(2,1)S(1)} %collective-permute-done.11), channel_id=1, source_target_pairs={{0,2},{2,4},{4,6},{6,8},{8,10},{10,12},{12,14},{14,16},{16,18},{18... | collective-permute-start | bytes 589832 | tf_op jit(solution)/shard_map/ppermute | solution.py:16
  148.7 14.2 %copy-start.11 = (bf16[192,4,128]{2,1,0:T(4,128)(2,1)}, bf16[192,4,128]{2,1,0:T(4,128)(2,1)S(1)}, u32[]{:S(2)}) copy-start(bf16[192,4,128]{2,1,0:T(4,128)(2,1)S(1)} %collective-permute-done.12) | copy-start | bytes 589828
  148.7 13.2 %collective-permute-start.13 = (bf16[192,4,128]{2,1,0:T(4,128)(2,1)S(1)}, bf16[192,4,128]{2,1,0:T(4,128)(2,1)}, u32[]{:S(2)}, u32[]{:S(2)}) collective-permute-start(bf16[192,4,128]{2,1,0:T(4,128)(2,1)S(1)} %collective-permute-done.12), channel_id=1, source_target_pairs={{0,2},{2,4},{4,6},{6,8},{8,10},{10,12},{12,14},{14,16},{16,18},{18... | collective-permute-start | bytes 589832 | tf_op jit(solution)/shard_map/ppermute | solution.py:16
  161.9 9.8 %collective-permute-start.14 = (bf16[192,4,128]{2,1,0:T(4,128)(2,1)}, bf16[192,4,128]{2,1,0:T(4,128)(2,1)}, u32[]{:S(2)}, u32[]{:S(2)}) collective-permute-start(bf16[192,4,128]{2,1,0:T(4,128)(2,1)} %collective-permute-done.13), channel_id=1, source_target_pairs={{0,2},{2,4},{4,6},{6,8},{8,10},{10,12},{12,14},{14,16},{16,18},{18... | collective-permute-start | bytes 589832 | tf_op jit(solution)/shard_map/ppermute | solution.py:16
  163.2 19.7 %copy-start.1 = (bf16[192,4,128]{2,1,0:T(4,128)(2,1)S(1)}, bf16[192,4,128]{2,1,0:T(4,128)(2,1)}, u32[]{:S(2)}) copy-start(bf16[192,4,128]{2,1,0:T(4,128)(2,1)} %copy-done) | copy-start | bytes 589828
  163.2 22.2 %copy-start.12 = (bf16[192,4,128]{2,1,0:T(4,128)(2,1)S(1)}, bf16[192,4,128]{2,1,0:T(4,128)(2,1)}, u32[]{:S(2)}) copy-start(bf16[192,4,128]{2,1,0:T(4,128)(2,1)} %copy-done.11) | copy-start | bytes 589828
  163.2 29.4 %copy-start.3 = (bf16[192,4,128]{2,1,0:T(4,128)(2,1)S(1)}, bf16[192,4,128]{2,1,0:T(4,128)(2,1)}, u32[]{:S(2)}) copy-start(bf16[192,4,128]{2,1,0:T(4,128)(2,1)} %copy-done.2) | copy-start | bytes 589828
  241.6 9.3 %copy-start.15 = (bf16[192,2048]{1,0:T(8,128)(2,1)S(1)}, bf16[192,2048]{1,0:T(8,128)(2,1)}, u32[]{:S(2)}) copy-start(bf16[192,2048]{1,0:T(8,128)(2,1)} %param.13) | copy-start | bytes 2359300
  241.6 10.5 %copy-start.16 = (f32[2048]{0:T(1024)S(1)}, f32[2048]{0:T(1024)}, u32[]{:S(2)}) copy-start(f32[2048]{0:T(1024)} %param.20) | copy-start | bytes 24580
  246.7 149.5 %all-gather.7.cloned.1.call-start = ((), (), s32[]{:S(2)}) async-start(), calls=%async_computation.4 | async-start | bytes 12255232 | tf_op jit(solution)/shard_map/all_gather | solution.py:133
  247.4 331.6 %all-gather.11.cloned.1.call-start = ((), (), s32[]{:S(2)}) async-start(), calls=%async_computation.6 | async-start | bytes 12255232 | tf_op jit(solution)/shard_map/all_gather | solution.py:136
  248.0 473.3 %all-gather.9.cloned.1.call-start = ((), (), s32[]{:S(2)}) async-start(), calls=%async_computation.5 | async-start | bytes 12255232 | tf_op jit(solution)/shard_map/all_gather | solution.py:134
  248.6 492.4 %reduce-scatter.5.cloned.1.call-start = ((), (), s32[]{:S(2)}) async-start(), calls=%async_computation.7 | async-start | bytes 1179648 | tf_op jit(solution)/shard_map/reduce_scatter | solution.py:137
Sparse Core Ops, SparseCore 0:
  81.0 76.5 all-gather.4
  246.8 4.0 reduce-scatter.2
  253.6 142.5 all-gather.6
  398.7 180.2 all-gather.10
  581.6 139.5 all-gather.8
  734.5 6.3 reduce-scatter.4
